TPU v7x, 32 devices: a whole 2x2x4 slice. The times are simulated.
32 devices in a mesh: sp: 8 (over z, x), tp: 4 (over y, core).
Axes of the slice: x: 2, y: 2, z: 4, core: 2. Of those that a mesh axis runs over, the one named last changes fastest.
Arguments:
- queries: bfloat16 [2048, 2048], P('sp', 'tp'), may hold values from -6 to 6
- keys: bfloat16 [2048, 1024], P('sp', 'tp'), may hold values from -6 to 6
- values: bfloat16 [2048, 1024], P('sp', 'tp'), may hold values from -6 to 6
- docs: int32 [2048], P('sp'), may hold values from 0 to 2, never falling along the last dimension, each value on 1 to 1280 neighbouring positions
- query_gain: float32 [64], replicated, may hold values from 0.5 to 8
- key_gain: float32 [64], replicated, may hold values from 0.5 to 8
- out_weight: bfloat16 [2048, 2048], P('tp'), may hold values from -0.125 to 0.125
- residual: bfloat16 [2048, 2048], P('sp', 'tp'), may hold values from -12 to 12
- norm_gain: float32 [2048], P('tp'), may hold values from 0.1 to 1.9
- routes: int32 [2048, 2], P('sp'), may hold values from 0 to 7, all different within a row; in each aligned block of 256 rows (0 to 255, 256 to 511, ...) at most 80 rows name the same one
- route_weight: float32 [2048, 2], P('sp'), may hold values from 0.1 to 1
- gate_weight: bfloat16 [8, 2048, 4096], P('sp', None, 'tp'), may hold values from -0.3125 to 0.3125
- up_weight: bfloat16 [8, 2048, 4096], P('sp', None, 'tp'), may hold values from -0.3125 to 0.3125
- down_weight: bfloat16 [8, 4096, 2048], P('sp', 'tp'), may hold values from -0.09375 to 0.09375
Outputs:
- mixed: bfloat16 [2048, 2048], P('sp', 'tp')
Inputs may be any that keep to these rules, and one draw needn't show every extreme that they name: `routes`: in each aligned block of 256 rows no expert is named by more than 80 rows, and 80 is reached in some block; a row names 2 different experts. `docs`: document numbers never fall along the sequence; a document holds at most 1280 positions.
All inputs are finite; a program needn't handle non-finite values.
Results may differ from a plain program's by a relative error of at most 0.028.
The roundings to bfloat16 on the way count: a program that leaves them out, or rounds other values in their place, can miss the bound.
Values may be sent and summed in bfloat16 or wider, within the bound.
A program may use at most 64 MiB of HBM per device.

v0:
```python
import jax
import jax.numpy as jnp
from jax import lax
from jax.sharding import PartitionSpec as P

GRID_W = 64
EPSILON = 1e-06
NEG_BIG = -1e30
ROTARY_BASE = 10000.0
CLAMP_LIMIT = 7.0
SIGMOID_SCALE = 1.702


def rope_tables(positions, head_dim):
    quarter = head_dim // 4
    freqs = ROTARY_BASE ** (-jnp.arange(quarter, dtype=jnp.float32) / quarter)
    row_pos = (positions // GRID_W).astype(jnp.float32)
    col_pos = (positions % GRID_W).astype(jnp.float32)
    angle = jnp.concatenate([row_pos[:, None] * freqs, col_pos[:, None] * freqs], axis=1)
    return (jnp.cos(angle), jnp.sin(angle))


def norm_rotate(heads, gain, cosine_table, sine_table):
    entries = heads.astype(jnp.float32)
    entries = (
        entries * lax.rsqrt(jnp.mean(entries * entries, axis=-1, keepdims=True) + EPSILON) * gain
    )
    pairs = entries.reshape(entries.shape[:-1] + (entries.shape[-1] // 2, 2))
    first = pairs[..., 0]
    second = pairs[..., 1]
    cos_rows = cosine_table[:, None, :]
    sin_rows = sine_table[:, None, :]
    turned = jnp.stack(
        [first * cos_rows - second * sin_rows, first * sin_rows + second * cos_rows], axis=-1
    )
    return turned.reshape(heads.shape).astype(jnp.bfloat16)


def clamped_unit(gate_pre, up_pre):
    bounded = jnp.minimum(gate_pre, CLAMP_LIMIT)
    linear = jnp.clip(up_pre, -CLAMP_LIMIT, CLAMP_LIMIT)
    return (bounded * jax.nn.sigmoid(SIGMOID_SCALE * bounded) * (linear + 1.0)).astype(jnp.bfloat16)


def block_length(length):
    block_size = length
    while block_size > 2048 and block_size % 2 == 0:
        block_size = block_size // 2
    return block_size


def softmax_update(running, inputs, query_rot, own_tags, score_scale):
    row_peak, denominator, carried = running
    key_block, value_block, tag_block = inputs
    scores = (
        jnp.einsum("tkgd,pkd->tkgp", query_rot, key_block, preferred_element_type=jnp.float32)
        * score_scale
    )
    allowed = own_tags[:, None, None, None] == tag_block[None, None, None, :]
    scores = jnp.where(allowed, scores, NEG_BIG)
    new_peak = jnp.maximum(row_peak, jnp.max(scores, axis=-1))
    weights = jnp.where(allowed, jnp.exp(scores - new_peak[..., None]), 0.0)
    factor = jnp.exp(row_peak - new_peak)
    denominator = denominator * factor + jnp.sum(weights, axis=-1)
    carried = carried * factor[..., None] + jnp.einsum(
        "tkgp,pkd->tkgd",
        weights.astype(jnp.bfloat16),
        value_block,
        preferred_element_type=jnp.float32,
    )
    return (new_peak, denominator, carried)


def per_device(
    queries,
    keys,
    values,
    docs,
    query_gain,
    key_gain,
    out_weight,
    residual,
    norm_gain,
    routes,
    route_weight,
    gate_weight,
    up_weight,
    down_weight,
):
    tokens = queries.shape[0]
    head_dim = query_gain.shape[0]
    query_heads = queries.shape[1] // head_dim
    pair_heads = keys.shape[1] // head_dim
    pair_width = keys.shape[1]
    positions = lax.axis_index("sp") * tokens + jnp.arange(tokens, dtype=jnp.int32)
    cosine_table, sine_table = rope_tables(positions, head_dim)
    query_rot = norm_rotate(
        queries.reshape(tokens, query_heads, head_dim), query_gain, cosine_table, sine_table
    )
    query_rot = query_rot.reshape(tokens, pair_heads, 2, head_dim)
    key_rot = norm_rotate(
        keys.reshape(tokens, pair_heads, head_dim), key_gain, cosine_table, sine_table
    )
    stacked = jnp.concatenate([key_rot.reshape(tokens, pair_width), values], axis=1)
    own_tags = docs.astype(jnp.bfloat16)
    score_scale = head_dim ** (-0.5)
    stat_shape = (tokens, pair_heads, 2)
    initial = (
        jnp.full(stat_shape, NEG_BIG, jnp.float32),
        jnp.zeros(stat_shape, jnp.float32),
        jnp.zeros(stat_shape + (head_dim,), jnp.float32),
    )
    pair_rows = lax.all_gather(stacked, "sp", axis=0, tiled=True)
    tag_rows = lax.all_gather(own_tags, "sp", axis=0, tiled=True)
    length = pair_rows.shape[0]
    block_size = block_length(length)
    blocks = length // block_size
    key_part = pair_rows[:, :pair_width].reshape(blocks, block_size, pair_heads, head_dim)
    value_part = pair_rows[:, pair_width:].reshape(blocks, block_size, pair_heads, head_dim)
    tag_part = tag_rows.reshape(blocks, block_size)

    def advance(carry_state, inputs):
        return (softmax_update(carry_state, inputs, query_rot, own_tags, score_scale), None)

    result, _ = lax.scan(advance, initial, (key_part, value_part, tag_part))
    row_peak, denominator, carried = result
    attended = (
        (carried / denominator[..., None])
        .astype(jnp.bfloat16)
        .reshape(tokens, query_heads * head_dim)
    )
    width_local = residual.shape[1]
    projected = lax.psum_scatter(
        lax.dot_general(
            out_weight, attended, (((0,), (1,)), ((), ())), preferred_element_type=jnp.float32
        ).astype(jnp.bfloat16),
        "tp",
        scatter_dimension=0,
        tiled=True,
    ).astype(jnp.float32)
    mixed_first = residual.astype(jnp.float32) + projected.T
    squares = lax.psum(jnp.sum(mixed_first * mixed_first, axis=1), "tp")
    full_width = width_local * lax.axis_size("tp")
    normed = (mixed_first * lax.rsqrt(squares / full_width + EPSILON)[:, None] * norm_gain).astype(
        jnp.bfloat16
    )
    experts = lax.axis_size("sp")
    top_count = routes.shape[1]
    capacity = max(2, 5 * tokens * top_count // (4 * experts))
    flat_routes = routes.reshape(-1)
    entries = flat_routes.shape[0]
    expert_ids = jnp.arange(experts, dtype=jnp.int32)
    onehot = (flat_routes[:, None] == expert_ids[None, :]).astype(jnp.int32)
    earlier = jnp.cumsum(onehot, axis=0) - onehot
    slot_index = jnp.sum(earlier * onehot, axis=1)
    slot_ids = jnp.arange(capacity, dtype=jnp.int32)
    matches = (flat_routes[:, None, None] == expert_ids[None, :, None]) & (
        slot_index[:, None, None] == slot_ids[None, None, :]
    )
    entry_ids = jnp.arange(entries, dtype=jnp.int32)
    source_entry = jnp.sum(jnp.where(matches, entry_ids[:, None, None], 0), axis=0)
    occupied = jnp.any(matches, axis=0)
    source_row = source_entry // top_count
    gate_local = gate_weight[0]
    up_local = up_weight[0]
    down_local = down_weight[0]
    model_width = gate_local.shape[0]
    outgoing = jnp.where(occupied[..., None], normed[source_row], jnp.zeros((), jnp.bfloat16))
    arrived = lax.all_to_all(outgoing, "sp", split_axis=0, concat_axis=0, tiled=True)
    sources = arrived.shape[0]
    flat_rows = arrived.reshape(-1, width_local)
    column_piece = lax.all_gather(flat_rows, "tp", axis=1, tiled=True)
    gate_pre = jnp.dot(column_piece, gate_local, preferred_element_type=jnp.float32)
    up_pre = jnp.dot(column_piece, up_local, preferred_element_type=jnp.float32)
    hidden = clamped_unit(gate_pre, up_pre)
    partial_value = jnp.dot(hidden, down_local, preferred_element_type=jnp.float32).reshape(
        sources, capacity, model_width
    )
    expert_out = lax.psum_scatter(
        partial_value.astype(jnp.bfloat16), "tp", scatter_dimension=2, tiled=True
    )
    returned = lax.all_to_all(expert_out, "sp", split_axis=0, concat_axis=0, tiled=True)
    lookup = flat_routes * capacity + slot_index
    picked = (
        returned.reshape(-1, width_local)[lookup]
        .reshape(tokens, top_count, width_local)
        .astype(jnp.float32)
    )
    routed = jnp.sum(route_weight[:, :, None] * picked, axis=1)
    return (mixed_first + routed).astype(jnp.bfloat16)


def solution(mesh):
    in_specs = (
        P("sp", "tp"),
        P("sp", "tp"),
        P("sp", "tp"),
        P("sp"),
        P(),
        P(),
        P("tp", None),
        P("sp", "tp"),
        P("tp"),
        P("sp", None),
        P("sp", None),
        P("sp", None, "tp"),
        P("sp", None, "tp"),
        P("sp", "tp", None),
    )
    out_specs = P("sp", "tp")
    return jax.shard_map(
        per_device, mesh=mesh, in_specs=in_specs, out_specs=out_specs, check_vma=False
    )
```

profile of v0, /device:TPU:0, one launch (start us, length us, event | category | flops | bytes accessed | tf_op | source)
XLA Modules:
  0.0 244.0 jit_solution(5147437151146860078)
XLA Ops:
  6.5 1.2 copy.40
  7.9 1.0 copy.41
  8.9 0.8 mul.239
  9.9 0.2 multiply_multiply_fusion.1
  10.1 0.3 subtract_convert_fusion.1
  10.5 0.3 pad_maximum_fusion.2
  10.8 0.7 pad_maximum_fusion
  11.6 0.7 convert_element_type.90
  12.3 22.4 %all-gather = bf16[8,1,256]{2,1,0:T(2,128)(2,1)S(1)} all-gather(bf16[1,1,256]{2,1,0:T(2,128)(2,1)S(1)} %reshape.382), channel_id=1, replica_groups=mesh['sp'=8,'tp'=4] {'sp'}, dimensions={0}, use_global_device_ids=true | all-gather | bytes 4608 | tf_op jit(solution)/shard_map/all_gather | solution.py:114
  34.7 1.1 copy.42
  35.8 0.3 reshape.363
  36.3 0.3 multiply_multiply_fusion
  36.6 0.7 subtract_convert_fusion
  37.2 0.6 pad_maximum_fusion.1
  38.0 0.4 broadcast_compare_fusion
  38.4 26.5 %all-gather.4.cloned.1.call-done = bf16[2048,512]{0,1:T(8,128)(2,1)} async-done(((bf16[256,512]{0,1:T(8,128)(2,1)}), bf16[2048,512]{0,1:T(8,128)(2,1)}) %all-gather.4.cloned.1.call-update) | async-done | bytes 2097168 | tf_op jit(solution)/shard_map/all_gather | solution.py:113
  64.8 1.7 fusion.46
  66.5 2.6 %fusion = (f32[256,4,2]{0,2,1:T(2,128)S(1)}, f32[4,2048,256,2]{2,1,3,0:T(8,128)S(1)}) fusion(pred[256,2048]{0,1:T(8,128)(4,1)S(1)} %broadcast_compare_fusion, bf16[2048,4,64,1]{0,2,3,1:T(8,128)(2,1)S(1)} %bitcast.120, bf16[256,4,2,64]{0,3,2,1:T(8,128)(2,1)S(1)} %convert_element_type.100), kind=kOutput, calls=%fused_computation.4 | convolution fusion | flops 549451776 | bytes 18620416 | tf_op jit(solution)/shard_map/while/body/eval_jaxpr/tkgd,pkd->tkgp/dot_general | solution.py:56
  69.1 4.0 %fusion.1 = f32[256,4,2]{0,2,1:T(2,128)S(1)} fusion(f32[4,2048,256,2]{2,1,3,0:T(8,128)S(1)} %get-tuple-element.45, f32[256,4,2]{0,2,1:T(2,128)S(1)} %broadcast_maximum_fusion, pred[256,2048]{0,1:T(8,128)(4,1)S(1)} %broadcast_compare_fusion), kind=kLoop, calls=%fused_computation.5 | loop fusion | flops 20969472 | bytes 17317888 | tf_op jit(solution)/shard_map/while/body/eval_jaxpr/reduce_sum | solution.py:64
  73.2 3.9 %fusion.28 = bf16[256,4,2,64]{0,3,2,1:T(8,128)(2,1)S(1)} fusion(bf16[2048,4,64,1]{0,2,3,1:T(8,128)(2,1)S(1)} %bitcast.119, f32[4,2048,256,2]{2,1,3,0:T(8,128)S(1)} %get-tuple-element.45, f32[256,4,2]{0,2,1:T(2,128)S(1)} %broadcast_maximum_fusion, pred[256,2048]{0,1:T(8,128)(4,1)S(1)} %broadcast_compare_fusion, f32[256,4,2]{0,2,1:T(2,128)S(1)} %get-tuple-element.41, ...), kind=kOutput, calls=%fused_computation.26 | convolution fusion | flops 558235648 | bytes 18636800 | tf_op jit(solution)/shard_map/while/body/eval_jaxpr/tkgp,pkd->tkgd/dot_general | solution.py:65
  77.2 1.7 fusion.15
  78.9 0.2 all-gather.6.cloned.1.call-start
  79.3 0.1 eq.89
  79.5 0.1 eq.85
  79.6 1.1 reduce-window.6
  80.8 0.2 slice_reduce_fusion
  81.2 0.3 fusion.18
  81.6 0.2 and_reduce_fusion
  81.8 20.3 %reduce-scatter.3.cloned.1.call-done = bf16[512,256]{0,1:T(8,128)(2,1)} async-done(((bf16[2048,256]{0,1:T(8,128)(2,1)}), bf16[512,256]{0,1:T(8,128)(2,1)}) %reduce-scatter.3.cloned.1.call-update) | async-done | bytes 262160 | tf_op jit(solution)/shard_map/reduce_scatter | solution.py:133
  102.1 1.1 multiply_reduce_fusion.1
  103.2 5.8 %psum.7 = f32[256]{0:T(256)S(1)} all-reduce(f32[256]{0:T(256)S(1)} %multiply_reduce_fusion.1), channel_id=1, replica_groups=mesh['sp'=8,'tp'=4] {'tp'}, use_global_device_ids=true, to_apply=%region_10.11 | all-reduce | flops 256 | bytes 2048 | tf_op jit(solution)/shard_map/psum | solution.py:142
  109.0 1.1 multiply_convert_fusion.1
  110.1 2.8 %gather_fusion = bf16[640,512]{1,0:T(8,128)(2,1)S(1)} fusion(bf16[256,512]{1,0:T(8,128)(2,1)S(1)} %multiply_convert_fusion.1, s32[1024]{0:T(1024)S(1)} %pad_clamp_fusion.1), kind=kCustom, calls=%fused_computation | custom fusion | bytes 1313280 | tf_op jit(solution)/shard_map/gather | solution.py:168
  112.9 0.2 broadcast_select_fusion
  113.0 23.1 %all_to_all.10 = bf16[8,80,512]{2,1,0:T(8,128)(2,1)} all-to-all(bf16[8,80,512]{2,1,0:T(8,128)(2,1)S(1)} %broadcast_select_fusion), channel_id=1, replica_groups=mesh['sp'=8,'tp'=4] {'sp'}, dimensions={0} | all-to-all | bytes 1310720 | tf_op jit(solution)/shard_map/all_to_all | solution.py:169
  136.2 23.3 %all-gather.6.cloned.1.call-done = bf16[640,2048]{1,0:T(8,128)(2,1)} async-done(((bf16[640,512]{1,0:T(8,128)(2,1)}), bf16[640,2048]{1,0:T(8,128)(2,1)}) %all-gather.6.cloned.1.call-update) | async-done | bytes 2621456 | tf_op jit(solution)/shard_map/all_gather | solution.py:172
  159.5 5.6 %fusion.8 = f32[640,1024]{1,0:T(8,128)S(1)} fusion(bf16[640,2048]{1,0:T(8,128)(2,1)} %all-gather.6.cloned.1.call-done, bf16[1,2048,1024]{2,1,0:T(8,128)(2,1)} %param.26), kind=kOutput, calls=%fused_computation.11 | convolution fusion | flops 2684354560 | bytes 9437184 | tf_op jit(solution)/shard_map/dot_general | solution.py:174
  165.1 3.5 %multiply_convert_fusion = bf16[640,1024]{1,0:T(8,128)(2,1)S(1)} fusion(f32[640,1024]{1,0:T(8,128)S(1)} %fusion.8, bf16[640,2048]{1,0:T(8,128)(2,1)S(1)} %copy-done.8, bf16[1,2048,1024]{2,1,0:T(8,128)(2,1)S(1)} %copy-done.6), kind=kOutput, calls=%fused_computation.16 | convolution fusion | flops 2690908160 | bytes 10747904 | tf_op jit(solution)/shard_map/dot_general | solution.py:173
  168.7 4.2 %fusion.12 = bf16[8,80,2048]{2,1,0:T(8,128)(2,1)} fusion(bf16[8,80,1024]{2,1,0:T(8,128)(2,1)S(1)} %bitcast.126, bf16[1,1024,2048]{2,1,0:T(8,128)(2,1)S(1)} %copy-done.7), kind=kOutput, calls=%fused_computation.15 | convolution fusion | flops 2685665280 | bytes 8126464 | tf_op jit(solution)/shard_map/dot_general | solution.py:176
  172.9 34.5 %reduce-scatter.5.cloned.1.call-done = bf16[8,80,512]{2,1,0:T(8,128)(2,1)} async-done(((bf16[8,80,2048]{2,1,0:T(8,128)(2,1)}), bf16[8,80,512]{2,1,0:T(8,128)(2,1)}) %reduce-scatter.5.cloned.1.call-update) | async-done | bytes 655376 | tf_op jit(solution)/shard_map/reduce_scatter | solution.py:179
  207.4 5.5 %all-to-all-start.1 = ((bf16[8,80,512]{2,1,0:T(8,128)(2,1)}), bf16[8,80,512]{2,1,0:T(8,128)(2,1)S(1)}, u32[]{:S(2)}, u32[]{:S(2)}) async-start(bf16[8,80,512]{2,1,0:T(8,128)(2,1)} %reduce-scatter.5.cloned.1.call-done), calls=%async_computation.3 | async-start | bytes 1310720 | tf_op jit(solution)/shard_map/all_to_all | solution.py:182
  212.9 0.1 copy.47
  213.1 0.1 mul.284
  213.4 16.7 %all-to-all-done.1 = bf16[8,80,512]{2,1,0:T(8,128)(2,1)S(1)} async-done(((bf16[8,80,512]{2,1,0:T(8,128)(2,1)}), bf16[8,80,512]{2,1,0:T(8,128)(2,1)S(1)}, u32[]{:S(2)}, u32[]{:S(2)}) %all-to-all-start.1) | async-done | bytes 655392 | tf_op jit(solution)/shard_map/all_to_all | solution.py:182
  230.0 2.6 %gather_fusion.1 = bf16[512,512]{1,0:T(8,128)(2,1)} fusion(bf16[640,512]{1,0:T(8,128)(2,1)S(1)} %bitcast.116, s32[1024]{0:T(1024)S(1)} %pad_clamp_fusion), kind=kCustom, calls=%fused_computation.1 | custom fusion | bytes 1050624 | tf_op jit(solution)/shard_map/gather | solution.py:185
  232.7 1.7 reshape.364
  234.4 1.3 multiply_reduce_fusion
  235.7 1.8 add_convert_fusion
  (57 shorter events, 1.6 us)
Async XLA Ops:
  6.5 70.7 %copy-start = (bf16[512,2048]{1,0:T(8,128)(2,1)S(1)}, bf16[512,2048]{1,0:T(8,128)(2,1)}, u32[]{:S(2)}) copy-start(bf16[512,2048]{1,0:T(8,128)(2,1)} %param.20) | copy-start | bytes 6291460
  6.5 29.6 %copy-start.5 = (f32[64]{0:T(128)S(1)}, f32[64]{0:T(128)}, u32[]{:S(2)}) copy-start(f32[64]{0:T(128)} %param.18) | copy-start | bytes 772
  6.5 58.3 %all-gather.4.cloned.1.call-start = ((), (), s32[]{:S(2)}) async-start(), calls=%async_computation.4 | async-start | bytes 2359296 | tf_op jit(solution)/shard_map/all_gather | solution.py:113
  11.6 90.5 %reduce-scatter.3.cloned.1.call-start = ((), (), s32[]{:S(2)}) async-start(), calls=%async_computation.5 | async-start | bytes 1310720 | tf_op jit(solution)/shard_map/reduce_scatter | solution.py:133
  77.2 2.0 copy-start.2
  77.2 24.9 %copy-start.1 = (bf16[256,512]{1,0:T(8,128)(2,1)S(1)}, bf16[256,512]{1,0:T(8,128)(2,1)}, u32[]{:S(2)}) copy-start(bf16[256,512]{1,0:T(8,128)(2,1)} %param.21) | copy-start | bytes 786436
  77.2 31.8 %copy-start.3 = (f32[512]{0:T(512)S(1)}, f32[512]{0:T(512)}, u32[]{:S(2)}) copy-start(f32[512]{0:T(512)} %param.22) | copy-start | bytes 6148
  78.9 80.6 %all-gather.6.cloned.1.call-start = ((), (), s32[]{:S(2)}) async-start(), calls=%async_computation.6 | async-start | bytes 3276800 | tf_op jit(solution)/shard_map/all_gather | solution.py:172
  136.1 71.3 %reduce-scatter.5.cloned.1.call-start = ((), (), s32[]{:S(2)}) async-start(), calls=%async_computation.7 | async-start | bytes 3276800 | tf_op jit(solution)/shard_map/reduce_scatter | solution.py:179
  159.5 5.6 %copy-start.6 = (bf16[1,2048,1024]{2,1,0:T(8,128)(2,1)S(1)}, bf16[1,2048,1024]{2,1,0:T(8,128)(2,1)}, u32[]{:S(2)}) copy-start(bf16[1,2048,1024]{2,1,0:T(8,128)(2,1)} %param.25) | copy-start | bytes 12582916
  159.5 5.6 %copy-start.8 = (bf16[640,2048]{1,0:T(8,128)(2,1)S(1)}, bf16[640,2048]{1,0:T(8,128)(2,1)}, u32[]{:S(2)}) copy-start(bf16[640,2048]{1,0:T(8,128)(2,1)} %all-gather.6.cloned.1.call-done) | copy-start | bytes 7864324
  165.1 3.6 %copy-start.7 = (bf16[1,1024,2048]{2,1,0:T(8,128)(2,1)S(1)}, bf16[1,1024,2048]{2,1,0:T(8,128)(2,1)}, u32[]{:S(2)}) copy-start(bf16[1,1024,2048]{2,1,0:T(8,128)(2,1)} %param.27) | copy-start | bytes 12582916
  172.9 40.3 %copy-start.4 = (f32[256,2]{0,1:T(2,128)S(1)}, f32[256,2]{0,1:T(2,128)}, u32[]{:S(2)}) copy-start(f32[256,2]{0,1:T(2,128)} %param.24) | copy-start | bytes 6148
  207.4 22.6 %all-to-all-start.1 = ((bf16[8,80,512]{2,1,0:T(8,128)(2,1)}), bf16[8,80,512]{2,1,0:T(8,128)(2,1)S(1)}, u32[]{:S(2)}, u32[]{:S(2)}) async-start(bf16[8,80,512]{2,1,0:T(8,128)(2,1)} %reduce-scatter.5.cloned.1.call-done), calls=%async_computation.3 | async-start | bytes 1310720 | tf_op jit(solution)/shard_map/all_to_all | solution.py:182
Sparse Core Ops, SparseCore 0:
  11.7 53.0 all-gather.3
  79.1 22.9 reduce-scatter.2
  136.2 23.2 all-gather.5
  173.0 34.3 reduce-scatter.4
where the time goes:
time: 245 us; the launch traced here: 244 us
  waiting for transfers between devices  121 us (49%)
  blocking collectives  51.2 us (21%)
  matrix products  21.6 us (9%)
  other arithmetic  15.9 us (6%)
  local copies, waits for them, and re-layouts  14.6 us (6%)
  between operations  13.6 us (6%)
  starting transfers between devices  5.82 us (2%)
    reduce_scatter x1, waiting for transfers between devices, per_device(): lax.psum_scatter(partial_value.astype(jnp.bfloat16), 'tp', scatter_dimens...  34.5 us
    all_gather x1, waiting for transfers between devices, per_device(): pair_rows = lax.all_gather(stacked, 'sp', axis=0, tiled=True)  26.5 us
    all_gather x1, waiting for transfers between devices, per_device(): column_piece = lax.all_gather(flat_rows, 'tp', axis=1, tiled=True)  23.3 us
    all_to_all x1, blocking collectives, per_device(): lax.all_to_all(outgoing, 'sp', split_axis=0, concat_axis=0, tiled=True)  23.1 us
    all_gather x1, blocking collectives, per_device(): tag_rows = lax.all_gather(own_tags, 'sp', axis=0, tiled=True)  22.4 us
    reduce_scatter x1, waiting for transfers between devices, per_device(): lax.psum_scatter(lax.dot_general(out_weight, attended, (((0,), (1,)), (()...  20.3 us
    all_to_all x1, waiting for transfers between devices, per_device(): lax.all_to_all(expert_out, 'sp', split_axis=0, concat_axis=0, tiled=True)  16.7 us
    psum x1, blocking collectives, per_device(): squares = lax.psum(jnp.sum(mixed_first * mixed_first, axis=1), 'tp')  5.76 us
  transfers between devices with their start and end apart: 5, of which 5 were waited for; matrix products, arithmetic and copies ran while one was open for 3% of the time, Pallas kernels for 0%

commit v1 on v0

--- a/solution.py
+++ b/solution.py
@@ -9,6 +9,24 @@
 ROTARY_BASE = 10000.0
 CLAMP_LIMIT = 7.0
 SIGMOID_SCALE = 1.702
+
+
+def sector_fill(panel, where_dim, target):
+    parts_out = panel.shape
+    even = panel.reshape(
+        *parts_out[:where_dim], target, parts_out[where_dim] // target, *parts_out[where_dim + 1 :]
+    )
+    return jnp.moveaxis(even, where_dim, 0)
+
+
+def tasks_apply(buf, on_dim):
+    buf = jnp.moveaxis(buf, 0, on_dim)
+    current_block = buf.shape
+    return buf.reshape(
+        *current_block[:on_dim],
+        current_block[on_dim] * current_block[on_dim + 1],
+        *current_block[on_dim + 2 :]
+    )
 
 
 def rope_tables(positions, head_dim):
@@ -179,7 +197,18 @@
     expert_out = lax.psum_scatter(
         partial_value.astype(jnp.bfloat16), "tp", scatter_dimension=2, tiled=True
     )
-    returned = lax.all_to_all(expert_out, "sp", split_axis=0, concat_axis=0, tiled=True)
+    s_next = lax.axis_size("sp")
+    everything = lax.axis_index("sp")
+    a_next, ready = (s_next, everything)
+    out_arr = sector_fill(expert_out, 0, a_next)
+    shelf = [out_arr[ready]]
+    for num in tuple(range(1, a_next)):
+        extra = out_arr[ready ^ num]
+        front = lax.ppermute(extra, "sp", [(no, no ^ num) for no in range(a_next)])
+        shelf.append(front)
+    val2 = jnp.stack(shelf)
+    out_arr = val2[ready ^ jnp.arange(a_next)]
+    returned = tasks_apply(out_arr, 0)
     lookup = flat_routes * capacity + slot_index
     picked = (
         returned.reshape(-1, width_local)[lookup]

time: 245 us -> 245 us (level)
  waiting for transfers between devices: 121 us -> 111 us
  starting transfers between devices: 5.82 us -> 11.6 us
  local copies, waits for them, and re-layouts: 14.6 us -> 19.2 us
    all_to_all x1 -> x0, waiting for transfers between devices: 16.7 us -> none  [per_device(): lax.all_to_all(expert_out, 'sp', split_axis=0, concat_axis=0, tiled=True)]
    ppermute x0 -> x7, starting transfers between devices: none -> 11.3 us  [per_device(): front = lax.ppermute(extra, 'sp', [(no, no ^ num) for no in range(a_next)])]
    ppermute x0 -> x7, waiting for transfers between devices: none -> 6.93 us  [per_device(): front = lax.ppermute(extra, 'sp', [(no, no ^ num) for no in range(a_next)])]
    all_to_all x1 -> x0, starting transfers between devices: 5.51 us -> none  [per_device(): lax.all_to_all(expert_out, 'sp', split_axis=0, concat_axis=0, tiled=True)]
    unnamed x25 -> x34, local copies, waits for them, and re-layouts: 3.58 us -> 5.34 us
  transfers between devices with their start and end apart: 5 -> 11, of which waited for: 5 -> 5; matrix products, arithmetic and copies ran while one was open for 3% -> 3% of each run, Pallas kernels for 0% -> 0%
where the time goes in v1:
time: 245 us; the launch traced here: 244 us
  waiting for transfers between devices  111 us (45%)
  blocking collectives  51.2 us (21%)
  matrix products  21.6 us (9%)
  local copies, waits for them, and re-layouts  19.2 us (8%)
  other arithmetic  15.9 us (6%)
  between operations  13.7 us (6%)
  starting transfers between devices  11.6 us (5%)
    reduce_scatter x1, waiting for transfers between devices, per_device(): lax.psum_scatter(partial_value.astype(jnp.bfloat16), 'tp', scatter_dimens...  33.9 us
    all_gather x1, waiting for transfers between devices, per_device(): pair_rows = lax.all_gather(stacked, 'sp', axis=0, tiled=True)  26.5 us
    all_gather x1, waiting for transfers between devices, per_device(): column_piece = lax.all_gather(flat_rows, 'tp', axis=1, tiled=True)  23.3 us
    all_to_all x1, blocking collectives, per_device(): lax.all_to_all(outgoing, 'sp', split_axis=0, concat_axis=0, tiled=True)  23.1 us
    all_gather x1, blocking collectives, per_device(): tag_rows = lax.all_gather(own_tags, 'sp', axis=0, tiled=True)  22.4 us
    reduce_scatter x1, waiting for transfers between devices, per_device(): lax.psum_scatter(lax.dot_general(out_weight, attended, (((0,), (1,)), (()...  20.3 us
    ppermute x7, starting transfers between devices, per_device(): front = lax.ppermute(extra, 'sp', [(no, no ^ num) for no in range(a_next)])  11.3 us
    ppermute x7, waiting for transfers between devices, per_device(): front = lax.ppermute(extra, 'sp', [(no, no ^ num) for no in range(a_next)])  6.93 us
  transfers between devices with their start and end apart: 11, of which 5 were waited for; matrix products, arithmetic and copies ran while one was open for 3% of the time, Pallas kernels for 0%

profile of v1, /device:TPU:0, one launch (start us, length us, event | category | flops | bytes accessed | tf_op | source)
XLA Modules:
  0.0 244.3 jit_solution(14502426641573958389)
XLA Ops:
  6.5 1.2 copy.40
  7.9 1.0 copy.41
  8.9 0.8 mul.239
  10.1 0.3 subtract_convert_fusion.1
  10.5 0.3 pad_maximum_fusion.2
  10.8 0.7 pad_maximum_fusion
  11.6 0.7 convert_element_type.90
  12.3 22.4 %all-gather = bf16[8,1,256]{2,1,0:T(2,128)(2,1)S(1)} all-gather(bf16[1,1,256]{2,1,0:T(2,128)(2,1)S(1)} %reshape.421), channel_id=1, replica_groups=mesh['sp'=8,'tp'=4] {'sp'}, dimensions={0}, use_global_device_ids=true | all-gather | bytes 4608 | tf_op jit(solution)/shard_map/all_gather | solution.py:132
  34.7 1.1 copy.42
  35.8 0.3 reshape.391
  36.6 0.7 subtract_convert_fusion
  37.2 0.6 pad_maximum_fusion.1
  38.0 0.4 broadcast_compare_fusion
  38.4 26.5 %all-gather.4.cloned.1.call-done = bf16[2048,512]{0,1:T(8,128)(2,1)} async-done(((bf16[256,512]{0,1:T(8,128)(2,1)}), bf16[2048,512]{0,1:T(8,128)(2,1)}) %all-gather.4.cloned.1.call-update) | async-done | bytes 2097168 | tf_op jit(solution)/shard_map/all_gather | solution.py:131
  64.8 1.7 fusion.47
  66.5 2.6 %fusion = (f32[256,4,2]{0,2,1:T(2,128)S(1)}, f32[4,2048,256,2]{2,1,3,0:T(8,128)S(1)}) fusion(pred[256,2048]{0,1:T(8,128)(4,1)S(1)} %broadcast_compare_fusion, bf16[2048,4,64,1]{0,2,3,1:T(8,128)(2,1)S(1)} %bitcast.139, bf16[256,4,2,64]{0,3,2,1:T(8,128)(2,1)S(1)} %convert_element_type.100), kind=kOutput, calls=%fused_computation.5 | convolution fusion | flops 549451776 | bytes 18620416 | tf_op jit(solution)/shard_map/while/body/eval_jaxpr/tkgd,pkd->tkgp/dot_general | solution.py:74
  69.1 4.0 %fusion.1 = f32[256,4,2]{0,2,1:T(2,128)S(1)} fusion(f32[4,2048,256,2]{2,1,3,0:T(8,128)S(1)} %get-tuple-element.52, f32[256,4,2]{0,2,1:T(2,128)S(1)} %broadcast_maximum_fusion, pred[256,2048]{0,1:T(8,128)(4,1)S(1)} %broadcast_compare_fusion), kind=kLoop, calls=%fused_computation.6 | loop fusion | flops 20969472 | bytes 17317888 | tf_op jit(solution)/shard_map/while/body/eval_jaxpr/reduce_sum | solution.py:82
  73.2 3.9 %fusion.28 = bf16[256,4,2,64]{0,3,2,1:T(8,128)(2,1)S(1)} fusion(bf16[2048,4,64,1]{0,2,3,1:T(8,128)(2,1)S(1)} %bitcast.138, f32[4,2048,256,2]{2,1,3,0:T(8,128)S(1)} %get-tuple-element.52, f32[256,4,2]{0,2,1:T(2,128)S(1)} %broadcast_maximum_fusion, pred[256,2048]{0,1:T(8,128)(4,1)S(1)} %broadcast_compare_fusion, f32[256,4,2]{0,2,1:T(2,128)S(1)} %get-tuple-element.48, ...), kind=kOutput, calls=%fused_computation.27 | convolution fusion | flops 558235648 | bytes 18636800 | tf_op jit(solution)/shard_map/while/body/eval_jaxpr/tkgp,pkd->tkgd/dot_general | solution.py:83
  77.2 1.7 fusion.15
  79.6 1.1 reduce-window.6
  81.2 0.3 fusion.18
  81.8 20.3 %reduce-scatter.3.cloned.1.call-done = bf16[512,256]{0,1:T(8,128)(2,1)} async-done(((bf16[2048,256]{0,1:T(8,128)(2,1)}), bf16[512,256]{0,1:T(8,128)(2,1)}) %reduce-scatter.3.cloned.1.call-update) | async-done | bytes 262160 | tf_op jit(solution)/shard_map/reduce_scatter | solution.py:151
  102.1 1.1 multiply_reduce_fusion.1
  103.2 5.8 %psum.7 = f32[256]{0:T(256)S(1)} all-reduce(f32[256]{0:T(256)S(1)} %multiply_reduce_fusion.1), channel_id=1, replica_groups=mesh['sp'=8,'tp'=4] {'tp'}, use_global_device_ids=true, to_apply=%region_10.11 | all-reduce | flops 256 | bytes 2048 | tf_op jit(solution)/shard_map/psum | solution.py:160
  109.0 1.1 multiply_convert_fusion.1
  110.1 2.8 %gather_fusion = bf16[640,512]{1,0:T(8,128)(2,1)S(1)} fusion(bf16[256,512]{1,0:T(8,128)(2,1)S(1)} %multiply_convert_fusion.1, s32[1024]{0:T(1024)S(1)} %pad_clamp_fusion.2), kind=kCustom, calls=%fused_computation | custom fusion | bytes 1313280 | tf_op jit(solution)/shard_map/gather | solution.py:186
  113.0 23.1 %all_to_all.5 = bf16[8,80,512]{2,1,0:T(8,128)(2,1)} all-to-all(bf16[8,80,512]{2,1,0:T(8,128)(2,1)S(1)} %broadcast_select_fusion), channel_id=1, replica_groups=mesh['sp'=8,'tp'=4] {'sp'}, dimensions={0} | all-to-all | bytes 1310720 | tf_op jit(solution)/shard_map/all_to_all | solution.py:187
  136.2 23.3 %all-gather.6.cloned.1.call-done = bf16[640,2048]{1,0:T(8,128)(2,1)} async-done(((bf16[640,512]{1,0:T(8,128)(2,1)}), bf16[640,2048]{1,0:T(8,128)(2,1)}) %all-gather.6.cloned.1.call-update) | async-done | bytes 2621456 | tf_op jit(solution)/shard_map/all_gather | solution.py:190
  159.5 5.6 %fusion.8 = f32[640,1024]{1,0:T(8,128)S(1)} fusion(bf16[640,2048]{1,0:T(8,128)(2,1)} %all-gather.6.cloned.1.call-done, bf16[1,2048,1024]{2,1,0:T(8,128)(2,1)} %param.26), kind=kOutput, calls=%fused_computation.12 | convolution fusion | flops 2684354560 | bytes 9437184 | tf_op jit(solution)/shard_map/dot_general | solution.py:192
  165.1 3.5 %multiply_convert_fusion = bf16[640,1024]{1,0:T(8,128)(2,1)S(1)} fusion(f32[640,1024]{1,0:T(8,128)S(1)} %fusion.8, bf16[640,2048]{1,0:T(8,128)(2,1)S(1)} %copy-done.9, bf16[1,2048,1024]{2,1,0:T(8,128)(2,1)S(1)} %copy-done.7), kind=kOutput, calls=%fused_computation.17 | convolution fusion | flops 2690908160 | bytes 10747904 | tf_op jit(solution)/shard_map/dot_general | solution.py:191
  168.7 4.2 %fusion.12 = bf16[8,80,2048]{2,1,0:T(8,128)(2,1)} fusion(bf16[8,80,1024]{2,1,0:T(8,128)(2,1)S(1)} %bitcast.146, bf16[1,1024,2048]{2,1,0:T(8,128)(2,1)S(1)} %copy-done.8), kind=kOutput, calls=%fused_computation.16 | convolution fusion | flops 2685665280 | bytes 8126464 | tf_op jit(solution)/shard_map/dot_general | solution.py:194
  173.5 33.9 %reduce-scatter.5.cloned.1.call-done = bf16[8,80,512]{2,1,0:T(8,128)(2,1)} async-done(((bf16[8,80,2048]{2,1,0:T(8,128)(2,1)}), bf16[8,80,512]{2,1,0:T(8,128)(2,1)}) %reduce-scatter.5.cloned.1.call-update) | async-done | bytes 655376 | tf_op jit(solution)/shard_map/reduce_scatter | solution.py:197
  207.4 1.2 constant_dynamic-slice_fusion
  208.6 1.5 collective-permute-start
  210.1 1.5 collective-permute-start.1
  211.6 0.5 collective-permute-start.2
  212.1 2.4 collective-permute-start.3
  214.5 1.4 collective-permute-start.4
  216.0 0.9 bitcast_dynamic-update-slice_fusion.7
  216.9 3.4 %collective-permute-start.5 = (bf16[1,80,512]{2,1,0:T(8,128)(2,1)S(1)}, bf16[1,80,512]{2,1,0:T(8,128)(2,1)S(1)}, u32[]{:S(2)}, u32[]{:S(2)}) collective-permute-start(bf16[1,80,512]{2,1,0:T(8,128)(2,1)S(1)} %get-tuple-element.24), channel_id=1, source_target_pairs={{0,24},{4,28},{8,16},{12,20},{16,8},{20,12},{24,0},{28,4},{1,25},{... | collective-permute-start | bytes 245768 | tf_op jit(solution)/shard_map/ppermute | solution.py:207
  220.3 0.6 collective-permute-start.6
  220.9 6.9 %collective-permute-done.4 = bf16[1,80,512]{2,1,0:T(8,128)(2,1)S(1)} collective-permute-done((bf16[1,80,512]{2,1,0:T(8,128)(2,1)S(1)}, bf16[1,80,512]{2,1,0:T(8,128)(2,1)S(1)}, u32[]{:S(2)}, u32[]{:S(2)}) %collective-permute-start.4) | collective-permute-done | bytes 81952 | tf_op jit(solution)/shard_map/ppermute | solution.py:207
  227.9 0.8 copy-done.2
  228.7 1.7 gather_fusion.1
  230.4 2.6 %gather_fusion.2 = bf16[512,512]{1,0:T(8,128)(2,1)} fusion(bf16[640,512]{1,0:T(8,128)(2,1)S(1)} %bitcast.135, s32[1024]{0:T(1024)S(1)} %pad_clamp_fusion), kind=kCustom, calls=%fused_computation.2 | custom fusion | bytes 1050624 | tf_op jit(solution)/shard_map/gather | solution.py:214
  233.0 1.7 reshape.392
  234.7 1.3 multiply_reduce_fusion
  236.0 1.8 add_convert_fusion
  (83 shorter events, 3.5 us)
Async XLA Ops:
  6.5 70.7 %copy-start = (bf16[512,2048]{1,0:T(8,128)(2,1)S(1)}, bf16[512,2048]{1,0:T(8,128)(2,1)}, u32[]{:S(2)}) copy-start(bf16[512,2048]{1,0:T(8,128)(2,1)} %param.20) | copy-start | bytes 6291460
  6.5 29.6 %copy-start.6 = (f32[64]{0:T(128)S(1)}, f32[64]{0:T(128)}, u32[]{:S(2)}) copy-start(f32[64]{0:T(128)} %param.18) | copy-start | bytes 772
  6.5 58.3 %all-gather.4.cloned.1.call-start = ((), (), s32[]{:S(2)}) async-start(), calls=%async_computation.3 | async-start | bytes 2359296 | tf_op jit(solution)/shard_map/all_gather | solution.py:131
  11.6 90.5 %reduce-scatter.3.cloned.1.call-start = ((), (), s32[]{:S(2)}) async-start(), calls=%async_computation.4 | async-start | bytes 1310720 | tf_op jit(solution)/shard_map/reduce_scatter | solution.py:151
  77.2 2.0 copy-start.3
  77.2 24.9 %copy-start.1 = (bf16[256,512]{1,0:T(8,128)(2,1)S(1)}, bf16[256,512]{1,0:T(8,128)(2,1)}, u32[]{:S(2)}) copy-start(bf16[256,512]{1,0:T(8,128)(2,1)} %param.21) | copy-start | bytes 786436
  77.2 31.8 %copy-start.4 = (f32[512]{0:T(512)S(1)}, f32[512]{0:T(512)}, u32[]{:S(2)}) copy-start(f32[512]{0:T(512)} %param.22) | copy-start | bytes 6148
  78.9 80.6 %all-gather.6.cloned.1.call-start = ((), (), s32[]{:S(2)}) async-start(), calls=%async_computation.5 | async-start | bytes 3276800 | tf_op jit(solution)/shard_map/all_gather | solution.py:190
  136.1 71.3 %reduce-scatter.5.cloned.1.call-start = ((), (), s32[]{:S(2)}) async-start(), calls=%async_computation.6 | async-start | bytes 3276800 | tf_op jit(solution)/shard_map/reduce_scatter | solution.py:197
  159.5 5.6 %copy-start.7 = (bf16[1,2048,1024]{2,1,0:T(8,128)(2,1)S(1)}, bf16[1,2048,1024]{2,1,0:T(8,128)(2,1)}, u32[]{:S(2)}) copy-start(bf16[1,2048,1024]{2,1,0:T(8,128)(2,1)} %param.25) | copy-start | bytes 12582916
  159.5 5.6 %copy-start.9 = (bf16[640,2048]{1,0:T(8,128)(2,1)S(1)}, bf16[640,2048]{1,0:T(8,128)(2,1)}, u32[]{:S(2)}) copy-start(bf16[640,2048]{1,0:T(8,128)(2,1)} %all-gather.6.cloned.1.call-done) | copy-start | bytes 7864324
  165.1 3.6 %copy-start.8 = (bf16[1,1024,2048]{2,1,0:T(8,128)(2,1)S(1)}, bf16[1,1024,2048]{2,1,0:T(8,128)(2,1)}, u32[]{:S(2)}) copy-start(bf16[1,1024,2048]{2,1,0:T(8,128)(2,1)} %param.27) | copy-start | bytes 12582916
  168.7 4.5 %copy-start.5 = (f32[256,2]{0,1:T(2,128)S(1)}, f32[256,2]{0,1:T(2,128)}, u32[]{:S(2)}) copy-start(f32[256,2]{0,1:T(2,128)} %param.24) | copy-start | bytes 6148
  208.6 8.3 %collective-permute-start = (bf16[1,80,512]{2,1,0:T(8,128)(2,1)S(1)}, bf16[1,80,512]{2,1,0:T(8,128)(2,1)S(1)}, u32[]{:S(2)}, u32[]{:S(2)}) collective-permute-start(bf16[1,80,512]{2,1,0:T(8,128)(2,1)S(1)} %get-tuple-element.40), channel_id=1, source_target_pairs={{0,4},{4,0},{8,12},{12,8},{16,20},{20,16},{24,28},{28,24},{1,5},{5... | collective-permute-start | bytes 245768 | tf_op jit(solution)/shard_map/ppermute | solution.py:207
  210.1 10.2 %collective-permute-start.1 = (bf16[1,80,512]{2,1,0:T(8,128)(2,1)S(1)}, bf16[1,80,512]{2,1,0:T(8,128)(2,1)S(1)}, u32[]{:S(2)}, u32[]{:S(2)}) collective-permute-start(bf16[1,80,512]{2,1,0:T(8,128)(2,1)S(1)} %get-tuple-element.38), channel_id=1, source_target_pairs={{0,8},{4,12},{8,0},{12,4},{16,24},{20,28},{24,16},{28,20},{1,9},{5... | collective-permute-start | bytes 245768 | tf_op jit(solution)/shard_map/ppermute | solution.py:207
  211.6 9.2 %collective-permute-start.2 = (bf16[1,80,512]{2,1,0:T(8,128)(2,1)S(1)}, bf16[1,80,512]{2,1,0:T(8,128)(2,1)S(1)}, u32[]{:S(2)}, u32[]{:S(2)}) collective-permute-start(bf16[1,80,512]{2,1,0:T(8,128)(2,1)S(1)} %get-tuple-element.36), channel_id=1, source_target_pairs={{0,12},{4,8},{8,4},{12,0},{16,28},{20,24},{24,20},{28,16},{1,13},{... | collective-permute-start | bytes 245768 | tf_op jit(solution)/shard_map/ppermute | solution.py:207
  212.1 8.7 %collective-permute-start.3 = (bf16[1,80,512]{2,1,0:T(8,128)(2,1)S(1)}, bf16[1,80,512]{2,1,0:T(8,128)(2,1)S(1)}, u32[]{:S(2)}, u32[]{:S(2)}) collective-permute-start(bf16[1,80,512]{2,1,0:T(8,128)(2,1)S(1)} %get-tuple-element.26), channel_id=1, source_target_pairs={{0,16},{4,20},{8,24},{12,28},{16,0},{20,4},{24,8},{28,12},{1,17},{... | collective-permute-start | bytes 245768 | tf_op jit(solution)/shard_map/ppermute | solution.py:207
  214.5 13.3 %collective-permute-start.4 = (bf16[1,80,512]{2,1,0:T(8,128)(2,1)S(1)}, bf16[1,80,512]{2,1,0:T(8,128)(2,1)S(1)}, u32[]{:S(2)}, u32[]{:S(2)}) collective-permute-start(bf16[1,80,512]{2,1,0:T(8,128)(2,1)S(1)} %get-tuple-element.25), channel_id=1, source_target_pairs={{0,20},{4,16},{8,28},{12,24},{16,4},{20,0},{24,12},{28,8},{1,21},{... | collective-permute-start | bytes 245768 | tf_op jit(solution)/shard_map/ppermute | solution.py:207
  216.9 10.9 %collective-permute-start.5 = (bf16[1,80,512]{2,1,0:T(8,128)(2,1)S(1)}, bf16[1,80,512]{2,1,0:T(8,128)(2,1)S(1)}, u32[]{:S(2)}, u32[]{:S(2)}) collective-permute-start(bf16[1,80,512]{2,1,0:T(8,128)(2,1)S(1)} %get-tuple-element.24), channel_id=1, source_target_pairs={{0,24},{4,28},{8,16},{12,20},{16,8},{20,12},{24,0},{28,4},{1,25},{... | collective-permute-start | bytes 245768 | tf_op jit(solution)/shard_map/ppermute | solution.py:207
  220.3 7.6 %collective-permute-start.6 = (bf16[1,80,512]{2,1,0:T(8,128)(2,1)S(1)}, bf16[1,80,512]{2,1,0:T(8,128)(2,1)S(1)}, u32[]{:S(2)}, u32[]{:S(2)}) collective-permute-start(bf16[1,80,512]{2,1,0:T(8,128)(2,1)S(1)} %get-tuple-element.23), channel_id=1, source_target_pairs={{0,28},{4,24},{8,20},{12,16},{16,12},{20,8},{24,4},{28,0},{1,29},{... | collective-permute-start | bytes 245768 | tf_op jit(solution)/shard_map/ppermute | solution.py:207
  227.9 0.8 copy-start.2
Sparse Core Ops, SparseCore 0:
  11.7 53.0 all-gather.3
  79.1 22.9 reduce-scatter.2
  136.2 23.2 all-gather.5
  173.0 34.3 reduce-scatter.4
